TPU v7x, 32 devices: a whole 2x2x4 slice. The times are simulated.
32 devices in a mesh: grp: 2 (over y), sp: 4 (over z), tp: 4 (over x, core).
Axes of the slice: x: 2, y: 2, z: 4, core: 2. Of those that a mesh axis runs over, the one named last changes fastest.
Arguments:
- query_rows: bfloat16 [1024, 1024], P(('grp', 'sp'), 'tp'), parts along dimension 0, may hold values from -12 to 12
- key_rows: bfloat16 [1024, 1024], P(('grp', 'sp'), 'tp'), parts along dimension 0, may hold values from -9 to 9
- value_rows: bfloat16 [1024, 1024], P(('grp', 'sp'), 'tp'), parts along dimension 0, may hold values from -6 to 6
- key_logit: bfloat16 [1024, 8], P(('grp', 'sp'), 'tp'), parts along dimension 0, as said below
- residual: bfloat16 [1024, 2048], P(('grp', 'sp')), parts along dimension 0, may hold values from -6 to 6
- out_weight: bfloat16 [1024, 2048], P('tp'), may hold values from -0.1875 to 0.1875
- mix_gain: float32 [2048], replicated, may hold values from 0.1 to 1.9
- ffn_gain: float32 [2048], replicated, may hold values from 0.1 to 1.9
- out_gain: float32 [2048], replicated, may hold values from 0.1 to 1.9
- gate_weight: bfloat16 [2048, 5120], P('sp', 'tp'), may hold values from -0.125 to 0.125
- up_weight: bfloat16 [2048, 5120], P('sp', 'tp'), may hold values from -0.125 to 0.125
- down_weight: bfloat16 [2048, 5120], P('sp', 'tp'), may hold values from -0.078125 to 0.078125
Outputs:
- layer_out: bfloat16 [1024, 2048], P(('grp', 'sp')), parts along dimension 0
There are 2 independent parts, one for each index of `grp`. A program takes and returns all parts, laid end to end along the dimension named above; an argument that names none is the same for every part. Nothing has to cross between parts.
Inputs may be any that keep to these rules, and one draw needn't show every extreme that they name: `key_logit`: log-odds offsets of the keys, all negative.
All inputs are finite; a program needn't handle non-finite values.
Results may differ from a plain program's by a relative error of at most 0.018.
Values may be sent and summed in bfloat16 or wider, within the bound.
A program may use at most 64 MiB of HBM per device.

v0:
```python
import functools

import jax
import jax.numpy as jnp
from jax import lax
from jax.experimental import pallas as pl
from jax.experimental.pallas import tpu as pltpu
from jax.sharding import PartitionSpec as P

epsilon = 1e-06
MESH = pl.DeviceIdType.MESH
F32 = jnp.float32
BF16 = jnp.bfloat16
LAG = 2
MOST_PIECES = 5


def normalize(rows):
    return rows * lax.rsqrt(jnp.mean(rows * rows, axis=-1, keepdims=True) + epsilon)


def each(count, body):
    if count <= 4:
        for i in range(count):
            body(i)
    else:

        def step(i, carry):
            body(i)
            return carry

        lax.fori_loop(0, count, step, 0)


def remote(src, dst, send, recv, axis, peer):
    return pltpu.make_async_remote_copy(
        src_ref=src,
        dst_ref=dst,
        send_sem=send,
        recv_sem=recv,
        device_id={axis: peer},
        device_id_type=MESH,
    )


def nt(a, b):
    return lax.dot_general(a, b, (((1,), (1,)), ((), ())), preferred_element_type=F32)


def kernel(
    S, TP, H, pieces,
    q, k, v, lg, mg, fg, og, res, ow, gw, uw, dw,
    out,
    kb, vb, lb, acc, run, owv, gwv, uwv, dwv, resv,
    hs, hr, mid, zs_sum, ns, na, tmp, gs, gr, hall, us, ur, zs, zr, oall,
    loc, kvs, kvr, hss, hrs, n1s, n1r, n2s, n2r, gss, grs, hars, hals, har,
    upss, upr, zss, zrs, oss, ors, outs,
):
    me, tp = lax.axis_index("sp"), lax.axis_index("tp")
    T = q.shape[0]
    hd = q.shape[1] // H
    D = out.shape[1]
    R, C = T // TP, D // S
    right, left = lax.rem(me + 1, S), lax.rem(me + S - 1, S)

    my_rows = pl.ds(pl.multiple_of(tp * R, R), R)
    loads = [
        pltpu.make_async_copy(a, b, loc.at[i])
        for i, (a, b) in enumerate(
            [(ow, owv), (res.at[my_rows], resv), (gw, gwv), (uw, uwv), (dw, dwv)]
        )
    ]
    for c in loads:
        c.start()

    barrier = pltpu.get_barrier_semaphore()
    for f in range(1, S):
        pl.semaphore_signal(barrier, inc=1, device_id={"sp": lax.rem(me + f, S)}, device_id_type=MESH)
    for f in range(1, TP):
        pl.semaphore_signal(barrier, inc=1, device_id={"tp": lax.rem(tp + f, TP)}, device_id_type=MESH)
    pl.semaphore_wait(barrier, S + TP - 2)

    def kv_copies(b, own):
        srcs = (k, v, lg) if own else (kb.at[b], vb.at[b], lb.at[b])
        return [
            remote(src, dst.at[b], kvs.at[b, i], kvr.at[b, i], "sp", right)
            for i, (src, dst) in enumerate(zip(srcs, (kb, vb, lb)))
        ]

    @pl.when(me < S - 1)
    def _():
        for c in kv_copies(me, True):
            c.start()

    rows = lax.broadcasted_iota(jnp.int32, (T, T), 0)
    cols = lax.broadcasted_iota(jnp.int32, (T, T), 1)
    causal = cols < rows
    later = (rows > cols).astype(F32)

    def block(kk, vv, ll, diag):
        for h in range(H):
            span = slice(h * hd, (h + 1) * hd)
            s = nt(q[:, span], kk[:, span]) * (hd**-0.5) + ll[h : h + 1, :]
            soft = jnp.log1p(jnp.exp(-jnp.abs(s)))
            keep = jnp.minimum(-s, 0.0) - soft
            logsig = jnp.minimum(s, 0.0) - soft
            if diag:
                keep = jnp.where(causal, keep, 0.0)
            within = jnp.dot(
                keep, later, preferred_element_type=F32, precision=lax.Precision.HIGHEST
            )
            stick = jnp.exp(logsig + within)
            if diag:
                stick = jnp.where(causal, stick, 0.0)
            part = jnp.dot(stick.astype(BF16), vv[:, span], preferred_element_type=F32)
            total = jnp.broadcast_to(jnp.sum(keep, axis=-1, keepdims=True), (T, hd))
            if diag:
                acc[h] = part
                run[h] = total
            else:
                acc[h] += jnp.exp(run[h]) * part
                run[h] += total

    block(k[...], v[...], lg[...], True)

    def earlier(i):
        b = me - 1 - i

        @pl.when(b >= 0)
        def _():
            for c in kv_copies(b, False):
                c.wait_recv()

            @pl.when(me < S - 1)
            def _():
                for c in kv_copies(b, False):
                    c.start()

            block(kb[b], vb[b], lb[b], False)

    each(S - 1, earlier)

    attended = jnp.concatenate([acc[h] for h in range(H)], axis=1).astype(BF16)
    loads[0].wait()
    width = 512 if D % 512 == 0 else D
    for c0 in range(0, D, width):
        piece = jnp.dot(attended, owv[:, c0 : c0 + width], preferred_element_type=F32)
        hs[:, :, c0 : c0 + width] = piece.astype(BF16).reshape(TP, R, width)

    def hp_copy(t, slot):
        return remote(hs.at[t], hr.at[slot], hss.at[t], hrs.at[slot], "tp", t)

    def others(count, own, body):
        def go(i):
            body(lax.rem(own + 1 + i, count))

        each(count - 1, go)

    others(TP, tp, lambda t: hp_copy(t, tp).start())
    mid[...] = hs[tp].astype(F32)

    def add_hp(t):
        hp_copy(t, t).wait_recv()
        mid[...] += hr[t].astype(F32)

    others(TP, tp, add_hp)
    loads[1].wait()
    mixed = mid[...].astype(BF16).astype(F32)
    middle = (resv[...].astype(F32) + mg[...] * normalize(mixed)).astype(BF16).astype(F32)
    mid[...] = middle
    normed = (fg[...] * normalize(middle)).astype(BF16)
    for j in range(S):
        ns[j] = normed[:, j * C : (j + 1) * C]

    def n1_copy(j, slot):
        return remote(ns.at[j], na.at[tp, slot], n1s.at[j], n1r.at[slot], "sp", j)

    def n2_copy(t, slot, s):
        return remote(na.at[tp, s], na.at[slot, s], n2s.at[t, s], n2r.at[slot, s], "tp", t)

    others(S, me, lambda j: n1_copy(j, me).start())
    na[tp, me] = ns[me]
    others(TP, tp, lambda t: n2_copy(t, tp, me).start())

    def pass_on(s):
        n1_copy(s, s).wait_recv()
        others(TP, tp, lambda t: n2_copy(t, tp, s).start())

    others(S, me, pass_on)
    for c in loads[2:4]:
        c.wait()

    def arrive(s):
        others(TP, tp, lambda t: remote(na.at[tp, s], na.at[t, s], n2s.at[t, s], n2r.at[t, s], "tp", t).wait_recv())

    W = gs.shape[-1]
    lag = LAG

    def partial(p, j):
        @pl.when(p == 0)
        def _():
            arrive(j)

        x = na[:, j].reshape(T, C)
        units = pl.ds(pl.multiple_of(p * W, W), W)
        tmp[0] = jnp.dot(x, gwv[:, units], preferred_element_type=F32)
        tmp[1] = jnp.dot(x, uwv[:, units], preferred_element_type=F32)

    def g_copy(p, j, slot, peer):
        return remote(gs.at[p, j], gr.at[p, slot], gss.at[p, j], grs.at[p, slot], "sp", peer)

    def chain(p, j, first, slot, peer):
        partial(p, j)

        @pl.when(first)
        def _():
            gs[p, j] = tmp[...].astype(BF16)

        @pl.when(jnp.logical_not(first))
        def _():
            g_copy(p, j, j, peer).wait_recv()
            gs[p, j] = (tmp[...] + gr[p, j].astype(F32)).astype(BF16)

        g_copy(p, j, slot, peer).start()

    def h_right(p, b):
        return remote(hall.at[p, b], hall.at[p, b], hars.at[p, b], har.at[p, b], "sp", right)

    def h_left(p, b):
        return remote(hall.at[p, b], hall.at[p, b], hals.at[p, b], har.at[p, b], "sp", left)

    def cut(at):
        return lax.div(at, S - 1), lax.rem(at, S - 1)

    def reduce_step(g):
        at_right = g - me * lag
        at_left = g - (S - 1 - me) * lag

        @pl.when((at_right >= 0) & (at_right < pieces * (S - 1)))
        def _():
            p, tau = cut(at_right)

            @pl.when(S - 1 - tau > me)
            def _():
                chain(p, S - 1 - tau, me == 0, S - 1 - tau, right)

        @pl.when((at_left >= 0) & (at_left < pieces * (S - 1)))
        def _():
            p, j = cut(at_left)

            @pl.when(j < me)
            def _():
                chain(p, j, me == S - 1, lax.select(j == me - 1, S, j), left)

    def finish(p):
        partial(p, me)

        @pl.when(me > 0)
        def _():
            g_copy(p, me, me, left).wait_recv()
            tmp[...] += gr[p, me].astype(F32)

        @pl.when(me < S - 1)
        def _():
            g_copy(p, me, S, right).wait_recv()
            tmp[...] += gr[p, S].astype(F32)

        gate = tmp[0]
        hall[p, me] = (gate / (1.0 + jnp.exp(-gate)) * tmp[1]).astype(BF16)

        @pl.when(me < S - 1)
        def _():
            h_right(p, me).start()

        @pl.when(me > 0)
        def _():
            h_left(p, me).start()

    def spread(p, i, then):
        lo, hi = me - 1 - i, me + 1 + i

        @pl.when(lo >= 0)
        def _():
            h_right(p, lo).wait_recv()

            @pl.when(me < S - 1)
            def _():
                h_right(p, lo).start()

            then(lo)

        @pl.when(hi < S)
        def _():
            h_left(p, hi).wait_recv()

            @pl.when(me > 0)
            def _():
                h_left(p, hi).start()

            then(hi)

    def step(g, carry):
        reduce_step(g)
        at = g - (S - 1) * lag
        p, tau = cut(at)

        @pl.when((at >= 0) & (tau == 0) & (p < pieces))
        def _():
            finish(p)

        def gather(i, carry):
            at_i = at - (i + 1) * lag
            p, tau = cut(at_i)

            @pl.when((at_i >= 0) & (tau == 0) & (p < pieces - 1))
            def _():
                spread(p, i, lambda b: None)

            return carry

        return lax.fori_loop(0, S - 1, gather, carry)

    steps = (S - 1) * (lag + max(pieces - 1, pieces - 2 + lag)) + 1
    lax.fori_loop(0, steps, step, 0)

    def up_copy(t, slot, b):
        return remote(us.at[t, b], ur.at[slot, b], upss.at[t, b], upr.at[slot, b], "tp", t)

    def down(b):
        rows_b = jnp.concatenate([hall[p, b] for p in range(pieces)], axis=1)
        us[:, b] = nt(rows_b, dwv[...]).astype(BF16).reshape(TP, R, C)
        others(TP, tp, lambda t: up_copy(t, tp, b).start())

    def z_copy(b, slot):
        return remote(zs.at[b], zr.at[slot], zss.at[b], zrs.at[slot], "sp", b)

    def settle(b):
        def add(t):
            up_copy(t, t, b).wait_recv()
            zs_sum[...] += ur[t, b].astype(F32)

        zs_sum[...] = us[tp, b].astype(F32)
        others(TP, tp, add)
        zs[b] = zs_sum[...].astype(BF16)

        @pl.when(b != me)
        def _():
            z_copy(b, me).start()

    loads[4].wait()
    down(me)

    def last(i, carry):
        spread(pieces - 1, i, down)
        return carry

    lax.fori_loop(0, S - 1, last, 0)
    others(S, me, settle)
    settle(me)
    zr[me] = zs[me]
    others(S, me, lambda s: z_copy(s, s).wait_recv())
    ffn = jnp.concatenate([zr[s] for s in range(S)], axis=1).astype(F32)
    oall[tp] = (mid[...] + og[...] * normalize(ffn)).astype(BF16)

    def o_copy(t, slot):
        return remote(oall.at[tp], oall.at[slot], oss.at[t], ors.at[slot], "tp", t)

    def o_out(t):
        return pltpu.make_async_copy(
            oall.at[t], out.at[pl.ds(pl.multiple_of(t * R, R), R)], outs.at[t]
        )

    others(TP, tp, lambda t: o_copy(t, tp).start())
    o_out(tp).start()

    def o_in(t):
        remote(oall.at[tp], oall.at[t], oss.at[t], ors.at[t], "tp", t).wait_recv()
        o_out(t).start()

    others(TP, tp, o_in)
    each(TP, lambda t: o_out(t).wait())

    @pl.when(me < S - 1)
    def _():
        def sent(b):
            @pl.when(b <= me)
            def _():
                for c in kv_copies(b, False):
                    c.wait_send()
                each(pieces, lambda p: h_right(p, b).wait_send())

        each(S, sent)

    @pl.when(me > 0)
    def _():
        def sent(b):
            @pl.when(b >= me)
            def _():
                each(pieces, lambda p: h_left(p, b).wait_send())

        each(S, sent)

    def sp_sent(j):
        n1_copy(j, me).wait_send()
        z_copy(j, me).wait_send()
        each(pieces, lambda p: g_copy(p, j, j, right).wait_send())

    others(S, me, sp_sent)

    def tp_sent(t):
        hp_copy(t, tp).wait_send()
        o_copy(t, tp).wait_send()

        def inner(s):
            n2_copy(t, tp, s).wait_send()
            up_copy(t, tp, s).wait_send()

        each(S, inner)

    others(TP, tp, tp_sent)


def solution(mesh):
    S, TP = mesh.shape["sp"], mesh.shape["tp"]

    def shards(q, k, v, lg, res, ow, mg, fg, og, gw, uw, dw):
        T, H = lg.shape
        hw = q.shape[1]
        D = res.shape[1]
        C, U = gw.shape
        R = T // TP
        pieces = max([p for p in range(1, MOST_PIECES + 1) if U % (128 * p) == 0], default=1)
        W = U // pieces
        pad = -H % 8
        lgt = jnp.pad(lg.astype(F32).T, ((0, pad), (0, 0)))
        vm = pl.BlockSpec(memory_space=pltpu.VMEM)
        hb = pl.BlockSpec(memory_space=pl.ANY)
        dma = pltpu.SemaphoreType.DMA
        return pl.pallas_call(
            functools.partial(kernel, S, TP, H, pieces),
            out_shape=jax.ShapeDtypeStruct((T, D), BF16),
            in_specs=[vm] * 7 + [hb] * 5,
            out_specs=hb,
            scratch_shapes=[
                pltpu.VMEM((S, T, hw), BF16),
                pltpu.VMEM((S, T, hw), BF16),
                pltpu.VMEM((S,) + lgt.shape, F32),
                pltpu.VMEM((H, T, hw // H), F32),
                pltpu.VMEM((H, T, hw // H), F32),
                pltpu.VMEM(ow.shape, BF16),
                pltpu.VMEM(gw.shape, BF16),
                pltpu.VMEM(uw.shape, BF16),
                pltpu.VMEM(dw.shape, BF16),
                pltpu.VMEM((R, D), BF16),
                pltpu.VMEM((TP, R, D), BF16),
                pltpu.VMEM((TP, R, D), BF16),
                pltpu.VMEM((R, D), F32),
                pltpu.VMEM((R, C), F32),
                pltpu.VMEM((S, R, C), BF16),
                pltpu.VMEM((TP, S, R, C), BF16),
                pltpu.VMEM((2, T, W), F32),
                pltpu.VMEM((pieces, S, 2, T, W), BF16),
                pltpu.VMEM((pieces, S + 1, 2, T, W), BF16),
                pltpu.VMEM((pieces, S, T, W), BF16),
                pltpu.VMEM((TP, S, R, C), BF16),
                pltpu.VMEM((TP, S, R, C), BF16),
                pltpu.VMEM((S, R, C), BF16),
                pltpu.VMEM((S, R, C), BF16),
                pltpu.VMEM((TP, R, D), BF16),
                dma((5,)),
                dma((S, 3)),
                dma((S, 3)),
                dma((TP,)),
                dma((TP,)),
                dma((S,)),
                dma((S,)),
                dma((TP, S)),
                dma((TP, S)),
                dma((pieces, S)),
                dma((pieces, S + 1)),
                dma((pieces, S)),
                dma((pieces, S)),
                dma((pieces, S)),
                dma((TP, S)),
                dma((TP, S)),
                dma((S,)),
                dma((S,)),
                dma((TP,)),
                dma((TP,)),
                dma((TP,)),
            ],
            compiler_params=pltpu.CompilerParams(
                collective_id=0, has_side_effects=True, vmem_limit_bytes=67043328 - 2**20
            ),
        )(q, k, v, lgt, mg[None], fg[None], og[None], res, ow, gw, uw, dw)

    placed = (
        P(("grp", "sp"), "tp"),
        P(("grp", "sp"), "tp"),
        P(("grp", "sp"), "tp"),
        P(("grp", "sp"), "tp"),
        P(("grp", "sp"), None),
        P("tp", None),
        P(),
        P(),
        P(),
        P("sp", "tp"),
        P("sp", "tp"),
        P("sp", "tp"),
    )
    return jax.shard_map(
        shards, mesh=mesh, in_specs=placed, out_specs=P(("grp", "sp"), None), check_vma=False
    )
```

profile of v0, /device:TPU:1, one launch (start us, length us, event | category | flops | bytes accessed | tf_op | source)
XLA Modules:
  0.0 114.4 jit_solution(5704049129599492754)
XLA Ops:
  0.0 1.2 %pad_convert_fusion.lg = f32[8,128]{1,0:T(8,128)} fusion(bf16[2,128]{1,0:T(2,128)(2,1)} %bitcast.7), kind=kLoop, calls=%fused_computation | loop fusion | flops 1024 | bytes 4608 | tf_op jit(solution)/shard_map/jit(_pad)/pad | solution.py:435
  1.3 111.3 %shard_map.118 = bf16[128,2048]{1,0:T(8,128)(2,1)} custom-call(bf16[128,256]{1,0:T(8,128)(2,1)} %q.1, bf16[128,256]{1,0:T(8,128)(2,1)} %k.1, bf16[128,256]{1,0:T(8,128)(2,1)} %v.1, f32[8,128]{1,0:T(8,128)} %pad_convert_fusion.lg, f32[1,2048]{1,0:T(1,128)} %bitcast.4, f32[1,2048]{1,0:T(1,128)} %bitcast.5, f32[1,2048]{1,0:T(1,128)} %bitcast.6, ...), custom_call_target="tpu_custom_call" | custom-call | tf_op jit(solution)/shard_map/pallas_call | solution.py:439
  112.6 1.9 %copy.14 = bf16[128,2048]{1,0:T(8,128)(2,1)} copy(bf16[128,2048]{1,0:T(8,128)(2,1)} %shard_map.118) | data formatting | bytes 1048576
where the time goes:
time: 115 us; the launch traced here: 114 us
  Pallas kernels  111 us (97%)
  local copies, waits for them, and re-layouts  1.88 us (2%)
  other arithmetic  1.25 us (1%)
    pallas_call x1, Pallas kernels, shards(): pl.pallas_call(functools.partial(kernel, S, TP, H, pieces), out_shape=jax...  111 us

commit v1 on v0

--- a/solution.py
+++ b/solution.py
@@ -13,6 +13,12 @@
 BF16 = jnp.bfloat16
 LAG = 2
 MOST_PIECES = 5
+SPLIT_UP = 1
+FIRST_DOWN = ((0, 0), (0, 1), (1, 0))
+
+
+def EXTRA_ORDER(S):
+    return list(range(S))
 
 
 def normalize(rows):
@@ -420,8 +426,547 @@
     others(TP, tp, tp_sent)
 
 
+def gathered(
+    S, TP, H, base, extras,
+    q, k, v, lg, mg, fg, og, res, ow, gw, uw, dw,
+    out,
+    kb, vb, lb, acc, run, owv, resv, hs, hr, mid, xm, xn, gu, hid, dn, us, ur, zq, ov,
+    loc, kvs, kvr, hss, hrs, azs, azr, axs, axr, acs, acr, afs, afr,
+    gzs, gzr, gys, gyr, dzs, dzr, dys, dyr, hxs, hxr, hcs, hcr, hfs, hfr,
+    rss, rsr, oxs, oxr, ocs, ocr, ofs, ofr, outs,
+):
+    me, tp, g = lax.axis_index("sp"), lax.axis_index("tp"), lax.axis_index("grp")
+    T = q.shape[0]
+    hd = q.shape[1] // H
+    D = out.shape[1]
+    R, C = T // TP, D // S
+    NT = gu.shape[0]
+    half, Q = C // 2, C // TP
+    xpeer = lax.rem(tp + 2, TP)
+    cpeer = tp + 1 - 2 * lax.rem(tp, 2)
+    far = lax.rem(cpeer + 2, TP)
+
+    def count(i):
+        c = base
+        for p in extras:
+            c = c + jnp.where(i == p, 1, 0)
+        return c
+
+    def first(i):
+        c = i * base
+        for p in extras:
+            c = c + jnp.where(i > p, 1, 0)
+        return c
+
+    def tiles_of(i, body):
+        c = count(i)
+        for m in sorted({base, base + 1} if extras else {base}):
+
+            @pl.when(c == m)
+            def _(m=m):
+                body(m)
+
+    n_me = count(me)
+    my_rows = pl.ds(pl.multiple_of(tp * R, R), R)
+    load_ow = pltpu.make_async_copy(ow, owv, loc.at[0])
+    load_res = pltpu.make_async_copy(res.at[my_rows], resv, loc.at[1])
+    load_ow.start()
+    load_res.start()
+
+    def own_gu(w, kk):
+        lanes = pl.ds(pl.multiple_of((first(me) + kk) * 128, 128), 128)
+        rows = pl.ds(pl.multiple_of(me * C, C), C)
+        return pltpu.make_async_copy(
+            (gw, uw)[w].at[:, lanes], gu.at[kk, rows, pl.ds(w * 128, 128)], loc.at[2 + w * NT + kk]
+        )
+
+    def own_dn(m):
+        lanes = pl.ds(pl.multiple_of(first(me) * 128, 128), m * 128)
+        rows = pl.ds(pl.multiple_of(tp * Q, Q), Q)
+        to = pl.ds(pl.multiple_of(tp * (m * 128), 128), m * 128)
+        return pltpu.make_async_copy(dw.at[rows, lanes], dn.at[me, :, to], loc.at[2 + 2 * NT])
+
+    def with_tiles(body):
+        for kk in range(NT):
+
+            @pl.when(kk < n_me)
+            def _(kk=kk):
+                body(kk)
+
+    def load_own(kk):
+        own_gu(0, kk).start()
+        own_gu(1, kk).start()
+
+    with_tiles(load_own)
+    tiles_of(me, lambda m: own_dn(m).start())
+
+    barrier = pltpu.get_barrier_semaphore()
+
+    def greet(i):
+        for f in range(TP):
+
+            @pl.when((i != 0) | (f != 0))
+            def _(f=f):
+                pl.semaphore_signal(
+                    barrier,
+                    inc=1,
+                    device_id={"sp": lax.rem(me + i, S), "tp": lax.rem(tp + f, TP)},
+                    device_id_type=MESH,
+                )
+
+    for i in range(S):
+        greet(i)
+    pl.semaphore_signal(barrier, inc=1, device_id={"grp": 1 - g}, device_id_type=MESH)
+    pl.semaphore_wait(barrier, S * TP)
+
+    def planes(body, up=True, down=True):
+        for f in range(S - 1):
+            if up:
+
+                @pl.when(S - 1 - f > me)
+                def _(f=f):
+                    body(S - 1 - f)
+
+            if down:
+
+                @pl.when(f < me)
+                def _(f=f):
+                    body(f)
+
+    def near(body):
+        for d in range(1, S):
+
+            @pl.when(me - d >= 0)
+            def _(d=d):
+                body(me - d)
+
+            @pl.when(me + d < S)
+            def _(d=d):
+                body(me + d)
+
+    def kv_copies(b, dst):
+        return [
+            remote(src, to.at[b], kvs.at[dst, i], kvr.at[b, i], "sp", dst)
+            for i, (src, to) in enumerate(zip((k, v, lg), (kb, vb, lb)))
+        ]
+
+    def send_kv(i):
+        for c in kv_copies(me, i):
+            c.start()
+
+    planes(send_kv, down=False)
+
+    def gz_copy(w, i, kk, src, dst):
+        lanes = pl.ds(pl.multiple_of((first(i) + kk) * 128, 128), 128)
+        rows = pl.ds(pl.multiple_of(src * C + g * half, half), half)
+        return remote(
+            (gw, uw)[w].at[pl.ds(pl.multiple_of(g * half, half), half), lanes],
+            gu.at[kk, rows, pl.ds(w * 128, 128)],
+            gzs.at[w, i, kk],
+            gzr.at[w, src, kk],
+            "sp",
+            dst,
+        )
+
+    def gy_copy(j, kk, h):
+        r = gu.at[kk, pl.ds(pl.multiple_of(j * C + h * half, half), half)]
+        return remote(r, r, gys.at[j, kk], gyr.at[j, kk], "grp", 1 - g)
+
+    def send_gu(w, kk, **sides):
+        def one(i):
+            @pl.when(kk < count(i))
+            def _():
+                gz_copy(w, i, kk, me, i).start()
+
+        planes(one, **sides)
+
+    def dz_copy(i, t, src, st, m):
+        lanes = pl.ds(pl.multiple_of(first(i) * 128, 128), m * 128)
+        rows = pl.ds(pl.multiple_of(t * Q + g * (Q // 2), Q // 2), Q // 2)
+        return pltpu.make_async_remote_copy(
+            src_ref=dw.at[rows, lanes],
+            dst_ref=dn.at[
+                src,
+                pl.ds(pl.multiple_of(g * (Q // 2), Q // 2), Q // 2),
+                pl.ds(pl.multiple_of(st * (m * 128), 128), m * 128),
+            ],
+            send_sem=dzs.at[i, t],
+            recv_sem=dzr.at[src, st],
+            device_id={"sp": i, "tp": t},
+            device_id_type=MESH,
+        )
+
+    def dp_copy(t, st, m):
+        lanes = pl.ds(pl.multiple_of(first(me) * 128, 128), m * 128)
+        rows = pl.ds(pl.multiple_of(t * Q, Q), Q)
+        return remote(
+            dw.at[rows, lanes],
+            dn.at[me, :, pl.ds(pl.multiple_of(st * (m * 128), 128), m * 128)],
+            dzs.at[me, t],
+            dzr.at[me, st],
+            "tp",
+            t,
+        )
+
+    def dy_copy(j, h, m):
+        r = dn.at[j, pl.ds(pl.multiple_of(h * (Q // 2), Q // 2), Q // 2), pl.ds(0, TP * m * 128)]
+        return remote(r, r, dys.at[j], dyr.at[j], "grp", 1 - g)
+
+    def peers(body):
+        for f in range(1, TP):
+            body(lax.rem(tp + f, TP))
+
+    def send_dn(i):
+        def some(m):
+            for t in range(TP):
+                dz_copy(i, t, me, tp, m).start()
+
+        tiles_of(i, some)
+
+    for kk in range(SPLIT_UP):
+        for w in range(2):
+            send_gu(w, kk, down=False)
+    for kk, w in FIRST_DOWN:
+        send_gu(w, kk, up=False)
+
+    rows = lax.broadcasted_iota(jnp.int32, (T, T), 0)
+    cols = lax.broadcasted_iota(jnp.int32, (T, T), 1)
+    causal = cols < rows
+    later = (rows > cols).astype(F32)
+
+    def block(kk, vv, ll, diag):
+        for h in range(H):
+            span = slice(h * hd, (h + 1) * hd)
+            s = nt(q[:, span], kk[:, span]) * (hd**-0.5) + ll[h : h + 1, :]
+            soft = jnp.log1p(jnp.exp(-jnp.abs(s)))
+            keep = jnp.minimum(-s, 0.0) - soft
+            logsig = jnp.minimum(s, 0.0) - soft
+            if diag:
+                keep = jnp.where(causal, keep, 0.0)
+            within = jnp.dot(
+                keep, later, preferred_element_type=F32, precision=lax.Precision.HIGHEST
+            )
+            stick = jnp.exp(logsig + within)
+            if diag:
+                stick = jnp.where(causal, stick, 0.0)
+            part = jnp.dot(stick.astype(BF16), vv[:, span], preferred_element_type=F32)
+            total = jnp.broadcast_to(jnp.sum(keep, axis=-1, keepdims=True), (T, hd))
+            if diag:
+                acc[h] = part
+                run[h] = total
+            else:
+                acc[h] += jnp.exp(run[h]) * part
+                run[h] += total
+
+    block(k[...], v[...], lg[...], True)
+
+    def earlier(i):
+        b = me - 1 - i
+
+        @pl.when(b >= 0)
+        def _():
+            for c in kv_copies(b, me):
+                c.wait_recv()
+            block(kb[b], vb[b], lb[b], False)
+
+    each(S - 1, earlier)
+
+    attended = jnp.concatenate([acc[h] for h in range(H)], axis=1).astype(BF16)
+    load_ow.wait()
+    width = 512 if D % 512 == 0 else D
+    for c0 in range(0, D, width):
+        piece = jnp.dot(attended, owv[:, c0 : c0 + width], preferred_element_type=F32)
+        hs[:, :, c0 : c0 + width] = piece.astype(BF16).reshape(TP, R, width)
+
+    def hp_copy(t, slot):
+        return remote(hs.at[t], hr.at[slot], hss.at[t], hrs.at[slot], "tp", t)
+
+    peers(lambda t: hp_copy(t, tp).start())
+    mid[...] = hs[tp].astype(F32)
+
+    def add_hp(t):
+        hp_copy(t, t).wait_recv()
+        mid[...] += hr[t].astype(F32)
+
+    peers(add_hp)
+    load_res.wait()
+    mixed = mid[...].astype(BF16).astype(F32)
+    xm[me, my_rows] = (resv[...].astype(F32) + mg[...] * normalize(mixed)).astype(BF16)
+
+    def piece_of(j, t):
+        return xm.at[j, pl.ds(pl.multiple_of(t * R, R), R)]
+
+    def az_copy(j, dst):
+        return remote(piece_of(j, tp), piece_of(j, tp), azs.at[dst], azr.at[j], "sp", dst)
+
+    def ax_copy(j, t):
+        return remote(piece_of(j, t), piece_of(j, t), axs.at[j], axr.at[j], "tp", xpeer)
+
+    def ac_copy(j, t):
+        return remote(piece_of(j, t), piece_of(j, t), acs.at[j], acr.at[j], "tp", cpeer)
+
+    def af_copy(j, t):
+        return remote(piece_of(j, t), piece_of(j, t), afs.at[j], afr.at[j], "tp", cpeer)
+
+    planes(lambda i: az_copy(me, i).start())
+    ax_copy(me, tp).start()
+    ac_copy(me, tp).start()
+
+    for kk in range(NT):
+        for w in range(2):
+            if kk >= SPLIT_UP:
+                send_gu(w, kk, down=False)
+            if (kk, w) not in FIRST_DOWN:
+                send_gu(w, kk, up=False)
+    planes(send_dn)
+    tiles_of(me, lambda m: peers(lambda t: dp_copy(t, tp, m).start()))
+
+    def pass_gu(kk):
+        def one(j):
+            gz_copy(0, me, kk, j, j).wait_recv()
+            gz_copy(1, me, kk, j, j).wait_recv()
+            gy_copy(j, kk, g).start()
+
+        planes(one)
+
+    def spread(j):
+        az_copy(j, j).wait_recv()
+        ax_copy(j, tp).start()
+        ac_copy(j, tp).start()
+
+    def hand_on(j):
+        ax_copy(j, xpeer).wait_recv()
+        af_copy(j, xpeer).start()
+
+    def ready(j):
+        ac_copy(j, cpeer).wait_recv()
+        af_copy(j, far).wait_recv()
+        for r0 in range(0, T, R):
+            rows_f = xm[j, pl.ds(r0, R)].astype(F32)
+            at = pl.ds(pl.multiple_of(j * T + r0, R), R)
+            xn[at] = (fg[...] * normalize(rows_f)).astype(BF16)
+
+    pass_gu(0)
+    hand_on(me)
+    near(spread)
+    near(hand_on)
+    ready(me)
+    near(ready)
+
+    def hid_at(t, kk):
+        return hid.at[t * NT + kk]
+
+    def hx_copy(t, kk):
+        return remote(hid_at(t, kk), hid_at(t, kk), hxs.at[kk], hxr.at[kk], "tp", xpeer)
+
+    def hc_copy(t, kk):
+        return remote(hid_at(t, kk), hid_at(t, kk), hcs.at[kk], hcr.at[kk], "tp", cpeer)
+
+    def hf_copy(t, kk):
+        return remote(hid_at(t, kk), hid_at(t, kk), hfs.at[kk], hfr.at[kk], "tp", cpeer)
+
+    def tile(kk):
+        if kk > 0:
+            pass_gu(kk)
+        own_gu(0, kk).wait()
+        own_gu(1, kk).wait()
+        planes(lambda j: gy_copy(j, kk, 1 - g).wait_recv())
+        both = jnp.dot(xn[...], gu[kk], preferred_element_type=F32)
+        gate, up = both[:, :128], both[:, 128:]
+        hid[tp * NT + kk] = (gate / (1.0 + jnp.exp(-gate)) * up).astype(BF16)
+        hx_copy(tp, kk).start()
+        hc_copy(tp, kk).start()
+
+    with_tiles(tile)
+
+    def pass_tile(kk):
+        hx_copy(xpeer, kk).wait_recv()
+        hf_copy(xpeer, kk).start()
+
+    with_tiles(pass_tile)
+
+    def pass_dn(j):
+        def some(m):
+            for st in range(TP):
+                dz_copy(me, tp, j, st, m).wait_recv()
+            dy_copy(j, g, m).start()
+
+        tiles_of(me, some)
+
+    near(pass_dn)
+
+    def hid_ready(kk):
+        hc_copy(cpeer, kk).wait_recv()
+        hf_copy(far, kk).wait_recv()
+
+    with_tiles(hid_ready)
+
+    def rs_copy(j, dst, src):
+        return remote(us.at[j, dst], ur.at[j, src], rss.at[j, dst], rsr.at[j, src], "sp", dst)
+
+    def down(j, own=False):
+        def some(m):
+            if own:
+                own_dn(m).wait()
+                peers(lambda t: dp_copy(tp, t, m).wait_recv())
+            else:
+                dy_copy(j, 1 - g, m).wait_recv()
+            x = jnp.concatenate(
+                [hid[t * NT + kk] for t in range(TP) for kk in range(m)], axis=1
+            )
+            us[j] = nt(x, dn[j, :, : TP * m * 128]).astype(BF16).reshape(S, T, Q)
+
+        tiles_of(me, some)
+        planes(lambda i: rs_copy(j, i, me).start())
+
+    down(me, True)
+    near(down)
+
+    def ox_copy(j, t):
+        return remote(zq.at[t, j], zq.at[t, j], oxs.at[j], oxr.at[j], "tp", xpeer)
+
+    def oc_copy(j, t):
+        return remote(zq.at[t, j], zq.at[t, j], ocs.at[j], ocr.at[j], "tp", cpeer)
+
+    def of_copy(j, t):
+        return remote(zq.at[t, j], zq.at[t, j], ofs.at[j], ofr.at[j], "tp", cpeer)
+
+    def settle(j):
+        planes(lambda i: rs_copy(j, i, i).wait_recv())
+        total = us[j, me].astype(F32)
+        for d in range(1, S):
+            total += ur[j, lax.rem(me + d, S)].astype(F32)
+        zq[tp, j] = total.astype(BF16)
+        ox_copy(j, tp).start()
+        oc_copy(j, tp).start()
+
+    for j in range(S):
+        settle(j)
+    for j in range(S):
+        ox_copy(j, xpeer).wait_recv()
+        of_copy(j, xpeer).start()
+    for j in range(S):
+        oc_copy(j, cpeer).wait_recv()
+        of_copy(j, far).wait_recv()
+
+    def o_out(r):
+        rows_r = pl.ds(r * R, R)
+        return pltpu.make_async_copy(ov.at[rows_r], out.at[rows_r], outs.at[r])
+
+    for r in range(TP):
+        rows_r = pl.ds(r * R, R)
+        ffn = jnp.concatenate(
+            [zq[t, j, rows_r] for j in range(S) for t in range(TP)], axis=1
+        ).astype(F32)
+        ov[rows_r] = (xm[me, rows_r].astype(F32) + og[...] * normalize(ffn)).astype(BF16)
+        o_out(r).start()
+
+    planes(lambda i: [c.wait_send() for c in kv_copies(me, i)], down=False)
+    peers(lambda t: hp_copy(t, tp).wait_send())
+    for j in range(S):
+        ax_copy(j, tp).wait_send()
+        ac_copy(j, tp).wait_send()
+        af_copy(j, xpeer).wait_send()
+        ox_copy(j, tp).wait_send()
+        oc_copy(j, tp).wait_send()
+        of_copy(j, xpeer).wait_send()
+        planes(lambda i: rs_copy(j, i, me).wait_send())
+
+    def sent(i):
+        az_copy(me, i).wait_send()
+        for kk in range(NT):
+            for w in range(2):
+
+                @pl.when(kk < count(i))
+                def _(kk=kk, w=w):
+                    gz_copy(w, i, kk, me, i).wait_send()
+
+        def some(m):
+            for t in range(TP):
+                dz_copy(i, t, me, tp, m).wait_send()
+
+        tiles_of(i, some)
+        tiles_of(me, lambda m: dy_copy(i, g, m).wait_send())
+
+    planes(sent)
+
+    def tile_sent(kk):
+        planes(lambda j: gy_copy(j, kk, g).wait_send())
+        hx_copy(tp, kk).wait_send()
+        hc_copy(tp, kk).wait_send()
+        hf_copy(xpeer, kk).wait_send()
+
+    with_tiles(tile_sent)
+    tiles_of(me, lambda m: peers(lambda t: dp_copy(t, tp, m).wait_send()))
+    for r in range(TP):
+        o_out(r).wait()
+
+
+def gathered_call(S, TP, q, k, v, lgt, H, mg, fg, og, res, ow, gw, uw, dw):
+    T, hw = q.shape
+    D = res.shape[1]
+    C, U = gw.shape
+    R, Q = T // TP, C // TP
+    base, extra = divmod(U // 128, S)
+    extras = EXTRA_ORDER(S)[:extra]
+    NT = base + (1 if extra else 0)
+    vm = pl.BlockSpec(memory_space=pltpu.VMEM)
+    hb = pl.BlockSpec(memory_space=pl.ANY)
+    dma = pltpu.SemaphoreType.DMA
+    pairs = lambda *shape: [dma(shape), dma(shape)]
+    return pl.pallas_call(
+        functools.partial(gathered, S, TP, H, base, extras),
+        out_shape=jax.ShapeDtypeStruct((T, D), BF16),
+        in_specs=[vm] * 7 + [hb] * 5,
+        out_specs=hb,
+        scratch_shapes=[
+            pltpu.VMEM((S, T, hw), BF16),
+            pltpu.VMEM((S, T, hw), BF16),
+            pltpu.VMEM((S,) + lgt.shape, F32),
+            pltpu.VMEM((H, T, hw // H), F32),
+            pltpu.VMEM((H, T, hw // H), F32),
+            pltpu.VMEM(ow.shape, BF16),
+            pltpu.VMEM((R, D), BF16),
+            pltpu.VMEM((TP, R, D), BF16),
+            pltpu.VMEM((TP, R, D), BF16),
+            pltpu.VMEM((R, D), F32),
+            pltpu.VMEM((S, T, D), BF16),
+            pltpu.VMEM((S * T, D), BF16),
+            pltpu.VMEM((NT, D, 256), BF16),
+            pltpu.VMEM((TP * NT, S * T, 128), BF16),
+            pltpu.VMEM((S, Q, TP * NT * 128), BF16),
+            pltpu.VMEM((S, S, T, Q), BF16),
+            pltpu.VMEM((S, S, T, Q), BF16),
+            pltpu.VMEM((TP, S, T, Q), BF16),
+            pltpu.VMEM((T, D), BF16),
+            dma((3 + 2 * NT,)),
+            *pairs(S, 3),
+            *pairs(TP),
+            *pairs(S),
+            *pairs(S),
+            *pairs(S),
+            *pairs(S),
+            *pairs(2, S, NT),
+            *pairs(S, NT),
+            *pairs(S, TP),
+            *pairs(S),
+            *pairs(NT),
+            *pairs(NT),
+            *pairs(NT),
+            *pairs(S, S),
+            *pairs(S),
+            *pairs(S),
+            *pairs(S),
+            dma((TP,)),
+        ],
+        compiler_params=pltpu.CompilerParams(
+            collective_id=0, has_side_effects=True, vmem_limit_bytes=67043328 - 2**20
+        ),
+    )(q, k, v, lgt, mg[None], fg[None], og[None], res, ow, gw, uw, dw)
+
+
 def solution(mesh):
-    S, TP = mesh.shape["sp"], mesh.shape["tp"]
+    S, TP, G = mesh.shape["sp"], mesh.shape["tp"], mesh.shape["grp"]
 
     def shards(q, k, v, lg, res, ow, mg, fg, og, gw, uw, dw):
         T, H = lg.shape
@@ -433,6 +978,8 @@
         W = U // pieces
         pad = -H % 8
         lgt = jnp.pad(lg.astype(F32).T, ((0, pad), (0, 0)))
+        if U % 128 == 0 and U // 128 >= S and C % (128 * TP) == 0 and T % (16 * TP) == 0 and (TP, G) == (4, 2):
+            return gathered_call(S, TP, q, k, v, lgt, H, mg, fg, og, res, ow, gw, uw, dw)
         vm = pl.BlockSpec(memory_space=pltpu.VMEM)
         hb = pl.BlockSpec(memory_space=pl.ANY)
         dma = pltpu.SemaphoreType.DMA

time: 115 us -> 119 us (1.035)
  Pallas kernels: 111 us -> 115 us
    pallas_call x1, Pallas kernels: 111 us -> 115 us  [gathered_call(): pl.pallas_call(functools.partial(gathered, S, TP, H, base, extras), out_s...]
where the time goes in v1:
time: 119 us
  Pallas kernels  115 us (97%)
  local copies, waits for them, and re-layouts  1.88 us (2%)
  other arithmetic  1.25 us (1%)
    pallas_call x1, Pallas kernels, gathered_call(): pl.pallas_call(functools.partial(gathered, S, TP, H, base, extras), out_s...  115 us

profile of v1, /device:TPU:1, one launch (start us, length us, event | category | flops | bytes accessed | tf_op | source)
XLA Modules:
  0.0 118.6 jit_solution(2451384453166634791)
XLA Ops:
  0.0 1.2 %pad_convert_fusion.lg = f32[8,128]{1,0:T(8,128)} fusion(bf16[2,128]{1,0:T(2,128)(2,1)} %bitcast.7), kind=kLoop, calls=%fused_computation | loop fusion | flops 1024 | bytes 4608 | tf_op jit(solution)/shard_map/jit(_pad)/pad | solution.py:980
  1.3 115.5 %shard_map.118 = bf16[128,2048]{1,0:T(8,128)(2,1)} custom-call(bf16[128,256]{1,0:T(8,128)(2,1)} %q.1, bf16[128,256]{1,0:T(8,128)(2,1)} %k.1, bf16[128,256]{1,0:T(8,128)(2,1)} %v.1, f32[8,128]{1,0:T(8,128)} %pad_convert_fusion.lg, f32[1,2048]{1,0:T(1,128)} %bitcast.4, f32[1,2048]{1,0:T(1,128)} %bitcast.5, f32[1,2048]{1,0:T(1,128)} %bitcast.6, ...), custom_call_target="tpu_custom_call" | custom-call | tf_op jit(solution)/shard_map/pallas_call | solution.py:917
  116.7 1.9 %copy.14 = bf16[128,2048]{1,0:T(8,128)(2,1)} copy(bf16[128,2048]{1,0:T(8,128)(2,1)} %shard_map.118) | data formatting | bytes 1048576

commit v2 on v1

--- a/solution.py
+++ b/solution.py
@@ -13,8 +13,7 @@
 BF16 = jnp.bfloat16
 LAG = 2
 MOST_PIECES = 5
-SPLIT_UP = 1
-FIRST_DOWN = ((0, 0), (0, 1), (1, 0))
+EARLY = 2
 
 
 def EXTRA_ORDER(S):
@@ -486,8 +485,8 @@
         to = pl.ds(pl.multiple_of(tp * (m * 128), 128), m * 128)
         return pltpu.make_async_copy(dw.at[rows, lanes], dn.at[me, :, to], loc.at[2 + 2 * NT])
 
-    def with_tiles(body):
-        for kk in range(NT):
+    def with_tiles(body, at=range(NT)):
+        for kk in at:
 
             @pl.when(kk < n_me)
             def _(kk=kk):
@@ -519,30 +518,19 @@
     pl.semaphore_signal(barrier, inc=1, device_id={"grp": 1 - g}, device_id_type=MESH)
     pl.semaphore_wait(barrier, S * TP)
 
-    def planes(body, up=True, down=True):
-        for f in range(S - 1):
+    def planes(body, up=True, down=True, at=range(1, S)):
+        for d in at:
+            if down:
+
+                @pl.when(me - d >= 0)
+                def _(d=d):
+                    body(me - d)
+
             if up:
 
-                @pl.when(S - 1 - f > me)
-                def _(f=f):
-                    body(S - 1 - f)
-
-            if down:
-
-                @pl.when(f < me)
-                def _(f=f):
-                    body(f)
-
-    def near(body):
-        for d in range(1, S):
-
-            @pl.when(me - d >= 0)
-            def _(d=d):
-                body(me - d)
-
-            @pl.when(me + d < S)
-            def _(d=d):
-                body(me + d)
+                @pl.when(me + d < S)
+                def _(d=d):
+                    body(me + d)
 
     def kv_copies(b, dst):
         return [
@@ -623,11 +611,9 @@
 
         tiles_of(i, some)
 
-    for kk in range(SPLIT_UP):
-        for w in range(2):
-            send_gu(w, kk, down=False)
-    for kk, w in FIRST_DOWN:
-        send_gu(w, kk, up=False)
+    for kk in range(min(EARLY, NT)):
+        send_gu(0, kk, up=False)
+        send_gu(1, kk, up=False)
 
     rows = lax.broadcasted_iota(jnp.int32, (T, T), 0)
     cols = lax.broadcasted_iota(jnp.int32, (T, T), 1)
@@ -683,6 +669,9 @@
 
     peers(lambda t: hp_copy(t, tp).start())
     mid[...] = hs[tp].astype(F32)
+    planes(lambda i: [c.wait_send() for c in kv_copies(me, i)], down=False)
+    send_gu(0, 0, down=False)
+    send_gu(1, 0, down=False)
 
     def add_hp(t):
         hp_copy(t, t).wait_recv()
@@ -696,8 +685,18 @@
     def piece_of(j, t):
         return xm.at[j, pl.ds(pl.multiple_of(t * R, R), R)]
 
-    def az_copy(j, dst):
-        return remote(piece_of(j, tp), piece_of(j, tp), azs.at[dst], azr.at[j], "sp", dst)
+    def az_copy(j, way):
+        r = piece_of(j, tp)
+        return remote(r, r, azs.at[way, j], azr.at[j], "sp", me + 1 if way else me - 1)
+
+    def ends(j, body):
+        @pl.when((j <= me) & (me < S - 1))
+        def _():
+            body(az_copy(j, 1))
+
+        @pl.when((j >= me) & (me > 0))
+        def _():
+            body(az_copy(j, 0))
 
     def ax_copy(j, t):
         return remote(piece_of(j, t), piece_of(j, t), axs.at[j], axr.at[j], "tp", xpeer)
@@ -708,29 +707,29 @@
     def af_copy(j, t):
         return remote(piece_of(j, t), piece_of(j, t), afs.at[j], afr.at[j], "tp", cpeer)
 
-    planes(lambda i: az_copy(me, i).start())
+    ends(me, lambda c: c.start())
     ax_copy(me, tp).start()
     ac_copy(me, tp).start()
 
-    for kk in range(NT):
-        for w in range(2):
-            if kk >= SPLIT_UP:
-                send_gu(w, kk, down=False)
-            if (kk, w) not in FIRST_DOWN:
-                send_gu(w, kk, up=False)
-    planes(send_dn)
-    tiles_of(me, lambda m: peers(lambda t: dp_copy(t, tp, m).start()))
-
-    def pass_gu(kk):
+    for w in range(2):
+        for kk in range(1, NT):
+            send_gu(w, kk, down=False)
+        for kk in range(EARLY, NT):
+            send_gu(w, kk, up=False)
+
+    def pass_gu(kk, **sides):
         def one(j):
             gz_copy(0, me, kk, j, j).wait_recv()
             gz_copy(1, me, kk, j, j).wait_recv()
             gy_copy(j, kk, g).start()
 
-        planes(one)
+        @pl.when(kk < n_me)
+        def _():
+            planes(one, **sides)
 
     def spread(j):
-        az_copy(j, j).wait_recv()
+        az_copy(j, 0).wait_recv()
+        ends(j, lambda c: c.start())
         ax_copy(j, tp).start()
         ac_copy(j, tp).start()
 
@@ -747,11 +746,19 @@
             xn[at] = (fg[...] * normalize(rows_f)).astype(BF16)
 
     pass_gu(0)
+    pass_gu(1, down=False)
     hand_on(me)
-    near(spread)
-    near(hand_on)
+    planes(spread, at=(1,))
+    planes(hand_on, at=(1,))
     ready(me)
-    near(ready)
+    planes(spread, at=(2,))
+    planes(hand_on, at=(2,))
+    planes(spread, at=range(3, S))
+    planes(send_dn)
+    tiles_of(me, lambda m: peers(lambda t: dp_copy(t, tp, m).start()))
+    planes(hand_on, at=range(3, S))
+    pass_gu(1, up=False)
+    planes(ready)
 
     def hid_at(t, kk):
         return hid.at[t * NT + kk]
@@ -766,8 +773,6 @@
         return remote(hid_at(t, kk), hid_at(t, kk), hfs.at[kk], hfr.at[kk], "tp", cpeer)
 
     def tile(kk):
-        if kk > 0:
-            pass_gu(kk)
         own_gu(0, kk).wait()
         own_gu(1, kk).wait()
         planes(lambda j: gy_copy(j, kk, 1 - g).wait_recv())
@@ -777,13 +782,17 @@
         hx_copy(tp, kk).start()
         hc_copy(tp, kk).start()
 
-    with_tiles(tile)
-
     def pass_tile(kk):
         hx_copy(xpeer, kk).wait_recv()
         hf_copy(xpeer, kk).start()
 
-    with_tiles(pass_tile)
+    with_tiles(tile, at=(0,))
+    for kk in range(2, NT):
+        pass_gu(kk)
+    with_tiles(tile, at=(1,))
+    with_tiles(pass_tile, at=(0,))
+    with_tiles(tile, at=range(2, NT))
+    with_tiles(pass_tile, at=range(1, NT))
 
     def pass_dn(j):
         def some(m):
@@ -793,13 +802,9 @@
 
         tiles_of(me, some)
 
-    near(pass_dn)
-
     def hid_ready(kk):
         hc_copy(cpeer, kk).wait_recv()
         hf_copy(far, kk).wait_recv()
-
-    with_tiles(hid_ready)
 
     def rs_copy(j, dst, src):
         return remote(us.at[j, dst], ur.at[j, src], rss.at[j, dst], rsr.at[j, src], "sp", dst)
@@ -819,8 +824,12 @@
         tiles_of(me, some)
         planes(lambda i: rs_copy(j, i, me).start())
 
+    planes(pass_dn, at=(1,))
+    with_tiles(hid_ready)
     down(me, True)
-    near(down)
+    for d in range(1, S):
+        planes(pass_dn, at=range(d + 1, min(d + 2, S)))
+        planes(down, at=(d,))
 
     def ox_copy(j, t):
         return remote(zq.at[t, j], zq.at[t, j], oxs.at[j], oxr.at[j], "tp", xpeer)
@@ -861,9 +870,9 @@
         ov[rows_r] = (xm[me, rows_r].astype(F32) + og[...] * normalize(ffn)).astype(BF16)
         o_out(r).start()
 
-    planes(lambda i: [c.wait_send() for c in kv_copies(me, i)], down=False)
     peers(lambda t: hp_copy(t, tp).wait_send())
     for j in range(S):
+        ends(j, lambda c: c.wait_send())
         ax_copy(j, tp).wait_send()
         ac_copy(j, tp).wait_send()
         af_copy(j, xpeer).wait_send()
@@ -873,7 +882,6 @@
         planes(lambda i: rs_copy(j, i, me).wait_send())
 
     def sent(i):
-        az_copy(me, i).wait_send()
         for kk in range(NT):
             for w in range(2):
 
@@ -942,7 +950,8 @@
             dma((3 + 2 * NT,)),
             *pairs(S, 3),
             *pairs(TP),
-            *pairs(S),
+            dma((2, S)),
+            dma((S,)),
             *pairs(S),
             *pairs(S),
             *pairs(S),

time: 119 us -> 104 us (0.87); the launches traced: 119 us -> 102 us
  Pallas kernels: 115 us -> 99.3 us
    pallas_call x1, Pallas kernels: 115 us -> 99.3 us  [gathered_call(): pl.pallas_call(functools.partial(gathered, S, TP, H, base, extras), out_s...]
where the time goes in v2:
time: 104 us; the launch traced here: 102 us
  Pallas kernels  99.3 us (95%)
  local copies, waits for them, and re-layouts  1.88 us (2%)
  other arithmetic  1.25 us (1%)
    pallas_call x1, Pallas kernels, gathered_call(): pl.pallas_call(functools.partial(gathered, S, TP, H, base, extras), out_s...  99.3 us

profile of v2, /device:TPU:1, one launch (start us, length us, event | category | flops | bytes accessed | tf_op | source)
XLA Modules:
  0.0 102.4 jit_solution(11646111462348286417)
XLA Ops:
  0.0 1.2 %pad_convert_fusion.lg = f32[8,128]{1,0:T(8,128)} fusion(bf16[2,128]{1,0:T(2,128)(2,1)} %bitcast.7), kind=kLoop, calls=%fused_computation | loop fusion | flops 1024 | bytes 4608 | tf_op jit(solution)/shard_map/jit(_pad)/pad | solution.py:989
  1.3 99.3 %shard_map.118 = bf16[128,2048]{1,0:T(8,128)(2,1)} custom-call(bf16[128,256]{1,0:T(8,128)(2,1)} %q.1, bf16[128,256]{1,0:T(8,128)(2,1)} %k.1, bf16[128,256]{1,0:T(8,128)(2,1)} %v.1, f32[8,128]{1,0:T(8,128)} %pad_convert_fusion.lg, f32[1,2048]{1,0:T(1,128)} %bitcast.4, f32[1,2048]{1,0:T(1,128)} %bitcast.5, f32[1,2048]{1,0:T(1,128)} %bitcast.6, ...), custom_call_target="tpu_custom_call" | custom-call | tf_op jit(solution)/shard_map/pallas_call | solution.py:925
  100.5 1.9 %copy.14 = bf16[128,2048]{1,0:T(8,128)(2,1)} copy(bf16[128,2048]{1,0:T(8,128)(2,1)} %shard_map.118) | data formatting | bytes 1048576

commit v3 on v2

--- a/solution.py
+++ b/solution.py
@@ -14,6 +14,10 @@
 LAG = 2
 MOST_PIECES = 5
 EARLY = 2
+
+
+def KV_ORDER(S):
+    return range(S - 1, 0, -1)
 
 
 def EXTRA_ORDER(S):
@@ -542,7 +546,7 @@
         for c in kv_copies(me, i):
             c.start()
 
-    planes(send_kv, down=False)
+    planes(send_kv, down=False, at=KV_ORDER(S))
 
     def gz_copy(w, i, kk, src, dst):
         lanes = pl.ds(pl.multiple_of((first(i) + kk) * 128, 128), 128)
@@ -596,9 +600,13 @@
             t,
         )
 
-    def dy_copy(j, h, m):
-        r = dn.at[j, pl.ds(pl.multiple_of(h * (Q // 2), Q // 2), Q // 2), pl.ds(0, TP * m * 128)]
-        return remote(r, r, dys.at[j], dyr.at[j], "grp", 1 - g)
+    def dy_copy(j, st, h, m):
+        r = dn.at[
+            j,
+            pl.ds(pl.multiple_of(h * (Q // 2), Q // 2), Q // 2),
+            pl.ds(pl.multiple_of(st * (m * 128), 128), m * 128),
+        ]
+        return remote(r, r, dys.at[j, st], dyr.at[j, st], "grp", 1 - g)
 
     def peers(body):
         for f in range(1, TP):
@@ -606,11 +614,12 @@
 
     def send_dn(i):
         def some(m):
-            for t in range(TP):
-                dz_copy(i, t, me, tp, m).start()
+            for f in range(TP):
+                dz_copy(i, lax.rem(tp + f, TP), me, tp, m).start()
 
         tiles_of(i, some)
 
+    tiles_of(me, lambda m: peers(lambda t: dp_copy(t, tp, m).start()))
     for kk in range(min(EARLY, NT)):
         send_gu(0, kk, up=False)
         send_gu(1, kk, up=False)
@@ -623,7 +632,7 @@
     def block(kk, vv, ll, diag):
         for h in range(H):
             span = slice(h * hd, (h + 1) * hd)
-            s = nt(q[:, span], kk[:, span]) * (hd**-0.5) + ll[h : h + 1, :]
+            s = nt(q[:, span], kk[:, span]) * (hd**-0.5) + ll[h : h + 1, :].astype(F32)
             soft = jnp.log1p(jnp.exp(-jnp.abs(s)))
             keep = jnp.minimum(-s, 0.0) - soft
             logsig = jnp.minimum(s, 0.0) - soft
@@ -685,18 +694,14 @@
     def piece_of(j, t):
         return xm.at[j, pl.ds(pl.multiple_of(t * R, R), R)]
 
-    def az_copy(j, way):
+    def az_copy(j, way, dst):
         r = piece_of(j, tp)
-        return remote(r, r, azs.at[way, j], azr.at[j], "sp", me + 1 if way else me - 1)
+        return remote(r, r, azs.at[way, j if way else dst], azr.at[j], "sp", dst)
 
     def ends(j, body):
         @pl.when((j <= me) & (me < S - 1))
         def _():
-            body(az_copy(j, 1))
-
-        @pl.when((j >= me) & (me > 0))
-        def _():
-            body(az_copy(j, 0))
+            body(az_copy(j, 1, me + 1))
 
     def ax_copy(j, t):
         return remote(piece_of(j, t), piece_of(j, t), axs.at[j], axr.at[j], "tp", xpeer)
@@ -708,14 +713,19 @@
         return remote(piece_of(j, t), piece_of(j, t), afs.at[j], afr.at[j], "tp", cpeer)
 
     ends(me, lambda c: c.start())
+    planes(lambda i: az_copy(me, 0, i).start(), up=False, at=range(S - 1, 0, -1))
     ax_copy(me, tp).start()
     ac_copy(me, tp).start()
+
+    def late_down():
+        for w in range(2):
+            for kk in range(EARLY, NT):
+                send_gu(w, kk, up=False)
 
     for w in range(2):
         for kk in range(1, NT):
             send_gu(w, kk, down=False)
-        for kk in range(EARLY, NT):
-            send_gu(w, kk, up=False)
+    pl.when(me < S - 1)(late_down)
 
     def pass_gu(kk, **sides):
         def one(j):
@@ -728,7 +738,7 @@
             planes(one, **sides)
 
     def spread(j):
-        az_copy(j, 0).wait_recv()
+        az_copy(j, 1, me).wait_recv()
         ends(j, lambda c: c.start())
         ax_copy(j, tp).start()
         ac_copy(j, tp).start()
@@ -745,19 +755,26 @@
             at = pl.ds(pl.multiple_of(j * T + r0, R), R)
             xn[at] = (fg[...] * normalize(rows_f)).astype(BF16)
 
+    def pass_late(at):
+        for kk in range(2, NT):
+            pass_gu(kk, at=at)
+
     pass_gu(0)
     pass_gu(1, down=False)
     hand_on(me)
     planes(spread, at=(1,))
     planes(hand_on, at=(1,))
+    pl.when(me == S - 1)(late_down)
     ready(me)
     planes(spread, at=(2,))
+    pass_late((1,))
     planes(hand_on, at=(2,))
     planes(spread, at=range(3, S))
+    pass_late((2,))
     planes(send_dn)
-    tiles_of(me, lambda m: peers(lambda t: dp_copy(t, tp, m).start()))
     planes(hand_on, at=range(3, S))
     pass_gu(1, up=False)
+    pass_late(range(3, S))
     planes(ready)
 
     def hid_at(t, kk):
@@ -786,21 +803,24 @@
         hx_copy(xpeer, kk).wait_recv()
         hf_copy(xpeer, kk).start()
 
+    def pass_dn(j, at=range(TP)):
+        def some(m):
+            for f in at:
+                st = lax.rem(tp + TP - f, TP)
+                dz_copy(me, tp, j, st, m).wait_recv()
+                dy_copy(j, st, g, m).start()
+
+        tiles_of(me, some)
+
     with_tiles(tile, at=(0,))
-    for kk in range(2, NT):
-        pass_gu(kk)
     with_tiles(tile, at=(1,))
+    planes(pass_dn, at=(1,))
     with_tiles(pass_tile, at=(0,))
     with_tiles(tile, at=range(2, NT))
-    with_tiles(pass_tile, at=range(1, NT))
-
-    def pass_dn(j):
-        def some(m):
-            for st in range(TP):
-                dz_copy(me, tp, j, st, m).wait_recv()
-            dy_copy(j, g, m).start()
-
-        tiles_of(me, some)
+    for f in range(TP):
+        if f == TP // 2:
+            with_tiles(pass_tile, at=range(1, NT))
+        planes(lambda j: pass_dn(j, (f,)), at=range(2, S))
 
     def hid_ready(kk):
         hc_copy(cpeer, kk).wait_recv()
@@ -815,7 +835,8 @@
                 own_dn(m).wait()
                 peers(lambda t: dp_copy(tp, t, m).wait_recv())
             else:
-                dy_copy(j, 1 - g, m).wait_recv()
+                for t in range(TP):
+                    dy_copy(j, t, 1 - g, m).wait_recv()
             x = jnp.concatenate(
                 [hid[t * NT + kk] for t in range(TP) for kk in range(m)], axis=1
             )
@@ -824,11 +845,9 @@
         tiles_of(me, some)
         planes(lambda i: rs_copy(j, i, me).start())
 
-    planes(pass_dn, at=(1,))
     with_tiles(hid_ready)
     down(me, True)
     for d in range(1, S):
-        planes(pass_dn, at=range(d + 1, min(d + 2, S)))
         planes(down, at=(d,))
 
     def ox_copy(j, t):
@@ -872,7 +891,7 @@
 
     peers(lambda t: hp_copy(t, tp).wait_send())
     for j in range(S):
-        ends(j, lambda c: c.wait_send())
+        pl.when(j <= me)(lambda: ends(j, lambda c: c.wait_send()))
         ax_copy(j, tp).wait_send()
         ac_copy(j, tp).wait_send()
         af_copy(j, xpeer).wait_send()
@@ -881,6 +900,8 @@
         of_copy(j, xpeer).wait_send()
         planes(lambda i: rs_copy(j, i, me).wait_send())
 
+    planes(lambda i: az_copy(me, 0, i).wait_send(), up=False)
+
     def sent(i):
         for kk in range(NT):
             for w in range(2):
@@ -894,7 +915,7 @@
                 dz_copy(i, t, me, tp, m).wait_send()
 
         tiles_of(i, some)
-        tiles_of(me, lambda m: dy_copy(i, g, m).wait_send())
+        tiles_of(me, lambda m: [dy_copy(i, t, g, m).wait_send() for t in range(TP)])
 
     planes(sent)
 
@@ -930,7 +951,7 @@
         scratch_shapes=[
             pltpu.VMEM((S, T, hw), BF16),
             pltpu.VMEM((S, T, hw), BF16),
-            pltpu.VMEM((S,) + lgt.shape, F32),
+            pltpu.VMEM((S,) + lgt.shape, lgt.dtype),
             pltpu.VMEM((H, T, hw // H), F32),
             pltpu.VMEM((H, T, hw // H), F32),
             pltpu.VMEM(ow.shape, BF16),
@@ -958,7 +979,7 @@
             *pairs(2, S, NT),
             *pairs(S, NT),
             *pairs(S, TP),
-            *pairs(S),
+            *pairs(S, TP),
             *pairs(NT),
             *pairs(NT),
             *pairs(NT),
@@ -988,7 +1009,7 @@
         pad = -H % 8
         lgt = jnp.pad(lg.astype(F32).T, ((0, pad), (0, 0)))
         if U % 128 == 0 and U // 128 >= S and C % (128 * TP) == 0 and T % (16 * TP) == 0 and (TP, G) == (4, 2):
-            return gathered_call(S, TP, q, k, v, lgt, H, mg, fg, og, res, ow, gw, uw, dw)
+            return gathered_call(S, TP, q, k, v, lg.T, H, mg, fg, og, res, ow, gw, uw, dw)
         vm = pl.BlockSpec(memory_space=pltpu.VMEM)
         hb = pl.BlockSpec(memory_space=pl.ANY)
         dma = pltpu.SemaphoreType.DMA

time: 104 us -> 94.1 us (0.905); the launches traced: 102 us -> 93.9 us
  Pallas kernels: 99.3 us -> 92.1 us
  other arithmetic: 1.25 us -> 0 us
    pallas_call x1, Pallas kernels: 99.3 us -> 92.1 us  [gathered_call(): pl.pallas_call(functools.partial(gathered, S, TP, H, base, extras), out_s...]
    pad x1 -> x0, other arithmetic: 1.25 us -> none  [shards(): lgt = jnp.pad(lg.astype(F32).T, ((0, pad), (0, 0)))]
where the time goes in v3:
time: 94.1 us; the launch traced here: 93.9 us
  Pallas kernels  92.1 us (98%)
  local copies, waits for them, and re-layouts  1.88 us (2%)
    pallas_call x1, Pallas kernels, gathered_call(): pl.pallas_call(functools.partial(gathered, S, TP, H, base, extras), out_s...  92.1 us

profile of v3, /device:TPU:1, one launch (start us, length us, event | category | flops | bytes accessed | tf_op | source)
XLA Modules:
  0.0 93.9 jit_solution(10476201012526381055)
XLA Ops:
  0.0 92.1 %shard_map.118 = bf16[128,2048]{1,0:T(8,128)(2,1)} custom-call(bf16[128,256]{1,0:T(8,128)(2,1)} %q.1, bf16[128,256]{1,0:T(8,128)(2,1)} %k.1, bf16[128,256]{1,0:T(8,128)(2,1)} %v.1, bf16[2,128]{1,0:T(2,128)(2,1)} %bitcast.7, f32[1,2048]{1,0:T(1,128)} %bitcast.4, f32[1,2048]{1,0:T(1,128)} %bitcast.5, f32[1,2048]{1,0:T(1,128)} %bitcast.6, ...), custom_call_target="tpu_custom_call" | custom-call | tf_op jit(solution)/shard_map/pallas_call | solution.py:946
  92.1 1.9 %copy.14 = bf16[128,2048]{1,0:T(8,128)(2,1)} copy(bf16[128,2048]{1,0:T(8,128)(2,1)} %shard_map.118) | data formatting | bytes 1048576

commit v4 on v3

--- a/solution.py
+++ b/solution.py
@@ -434,9 +434,9 @@
     q, k, v, lg, mg, fg, og, res, ow, gw, uw, dw,
     out,
     kb, vb, lb, acc, run, owv, resv, hs, hr, mid, xm, xn, gu, hid, dn, us, ur, zq, ov,
-    loc, kvs, kvr, hss, hrs, azs, azr, axs, axr, acs, acr, afs, afr,
-    gzs, gzr, gys, gyr, dzs, dzr, dys, dyr, hxs, hxr, hcs, hcr, hfs, hfr,
-    rss, rsr, oxs, oxr, ocs, ocr, ofs, ofr, outs,
+    loc, kvs, kvr, hss, hrs, azs, azr, axs, axr, acs, acr,
+    gzs, gzr, gys, gyr, dzs, dzr, dys, dyr, hxs, hxr, hcr,
+    rss, rsr, oxs, oxr, ocs, ocr, outs,
 ):
     me, tp, g = lax.axis_index("sp"), lax.axis_index("tp"), lax.axis_index("grp")
     T = q.shape[0]
@@ -476,18 +476,21 @@
     load_ow.start()
     load_res.start()
 
+    def drain(ref, sem):
+        remote(ref, ref, sem, sem, "tp", xpeer).wait_recv()
+
     def own_gu(w, kk):
         lanes = pl.ds(pl.multiple_of((first(me) + kk) * 128, 128), 128)
         rows = pl.ds(pl.multiple_of(me * C, C), C)
         return pltpu.make_async_copy(
-            (gw, uw)[w].at[:, lanes], gu.at[kk, rows, pl.ds(w * 128, 128)], loc.at[2 + w * NT + kk]
+            (gw, uw)[w].at[:, lanes], gu.at[kk, rows, pl.ds(w * 128, 128)], loc.at[3 + w * NT + kk]
         )
 
     def own_dn(m):
         lanes = pl.ds(pl.multiple_of(first(me) * 128, 128), m * 128)
         rows = pl.ds(pl.multiple_of(tp * Q, Q), Q)
         to = pl.ds(pl.multiple_of(tp * (m * 128), 128), m * 128)
-        return pltpu.make_async_copy(dw.at[rows, lanes], dn.at[me, :, to], loc.at[2 + 2 * NT])
+        return pltpu.make_async_copy(dw.at[rows, lanes], dn.at[me, :, to], loc.at[2])
 
     def with_tiles(body, at=range(NT)):
         for kk in at:
@@ -538,7 +541,7 @@
 
     def kv_copies(b, dst):
         return [
-            remote(src, to.at[b], kvs.at[dst, i], kvr.at[b, i], "sp", dst)
+            remote(src, to.at[b], kvs.at[dst, i // 2], kvr.at[b, i // 2], "sp", dst)
             for i, (src, to) in enumerate(zip((k, v, lg), (kb, vb, lb)))
         ]
 
@@ -554,15 +557,15 @@
         return remote(
             (gw, uw)[w].at[pl.ds(pl.multiple_of(g * half, half), half), lanes],
             gu.at[kk, rows, pl.ds(w * 128, 128)],
-            gzs.at[w, i, kk],
-            gzr.at[w, src, kk],
+            gzs.at[i, kk],
+            gzr.at[src, kk],
             "sp",
             dst,
         )
 
     def gy_copy(j, kk, h):
         r = gu.at[kk, pl.ds(pl.multiple_of(j * C + h * half, half), half)]
-        return remote(r, r, gys.at[j, kk], gyr.at[j, kk], "grp", 1 - g)
+        return remote(r, r, gys.at[kk], gyr.at[kk], "grp", 1 - g)
 
     def send_gu(w, kk, **sides):
         def one(i):
@@ -582,7 +585,7 @@
                 pl.ds(pl.multiple_of(g * (Q // 2), Q // 2), Q // 2),
                 pl.ds(pl.multiple_of(st * (m * 128), 128), m * 128),
             ],
-            send_sem=dzs.at[i, t],
+            send_sem=dzs.at[i],
             recv_sem=dzr.at[src, st],
             device_id={"sp": i, "tp": t},
             device_id_type=MESH,
@@ -594,8 +597,8 @@
         return remote(
             dw.at[rows, lanes],
             dn.at[me, :, pl.ds(pl.multiple_of(st * (m * 128), 128), m * 128)],
-            dzs.at[me, t],
-            dzr.at[me, st],
+            dzs.at[me],
+            dzr.at[me, 0],
             "tp",
             t,
         )
@@ -606,7 +609,7 @@
             pl.ds(pl.multiple_of(h * (Q // 2), Q // 2), Q // 2),
             pl.ds(pl.multiple_of(st * (m * 128), 128), m * 128),
         ]
-        return remote(r, r, dys.at[j, st], dyr.at[j, st], "grp", 1 - g)
+        return remote(r, r, dys.at[j], dyr.at[j], "grp", 1 - g)
 
     def peers(body):
         for f in range(1, TP):
@@ -614,8 +617,8 @@
 
     def send_dn(i):
         def some(m):
-            for f in range(TP):
-                dz_copy(i, lax.rem(tp + f, TP), me, tp, m).start()
+            for t in (tp, cpeer, xpeer, far):
+                dz_copy(i, t, me, tp, m).start()
 
         tiles_of(i, some)
 
@@ -660,8 +663,8 @@
 
         @pl.when(b >= 0)
         def _():
-            for c in kv_copies(b, me):
-                c.wait_recv()
+            drain(kb.at[pl.ds(0, 2)], kvr.at[b, 0])
+            drain(lb.at[0], kvr.at[b, 1])
             block(kb[b], vb[b], lb[b], False)
 
     each(S - 1, earlier)
@@ -674,16 +677,20 @@
         hs[:, :, c0 : c0 + width] = piece.astype(BF16).reshape(TP, R, width)
 
     def hp_copy(t, slot):
-        return remote(hs.at[t], hr.at[slot], hss.at[t], hrs.at[slot], "tp", t)
+        return remote(hs.at[t], hr.at[slot], hss.at[0], hrs.at[0], "tp", t)
 
     peers(lambda t: hp_copy(t, tp).start())
     mid[...] = hs[tp].astype(F32)
-    planes(lambda i: [c.wait_send() for c in kv_copies(me, i)], down=False)
+    planes(
+        lambda i: [drain(kb.at[pl.ds(0, 2)], kvs.at[i, 0]), drain(lb.at[0], kvs.at[i, 1])],
+        down=False,
+    )
     send_gu(0, 0, down=False)
     send_gu(1, 0, down=False)
 
+    drain(hr.at[pl.ds(0, TP - 1)], hrs.at[0])
+
     def add_hp(t):
-        hp_copy(t, t).wait_recv()
         mid[...] += hr[t].astype(F32)
 
     peers(add_hp)
@@ -704,13 +711,13 @@
             body(az_copy(j, 1, me + 1))
 
     def ax_copy(j, t):
-        return remote(piece_of(j, t), piece_of(j, t), axs.at[j], axr.at[j], "tp", xpeer)
+        return remote(piece_of(j, t), piece_of(j, t), axs.at[0], axr.at[j], "tp", xpeer)
 
     def ac_copy(j, t):
-        return remote(piece_of(j, t), piece_of(j, t), acs.at[j], acr.at[j], "tp", cpeer)
+        return remote(piece_of(j, t), piece_of(j, t), acs.at[0], acr.at[j], "tp", cpeer)
 
     def af_copy(j, t):
-        return remote(piece_of(j, t), piece_of(j, t), afs.at[j], afr.at[j], "tp", cpeer)
+        return remote(piece_of(j, t), piece_of(j, t), acs.at[0], acr.at[j], "tp", cpeer)
 
     ends(me, lambda c: c.start())
     planes(lambda i: az_copy(me, 0, i).start(), up=False, at=range(S - 1, 0, -1))
@@ -722,15 +729,11 @@
             for kk in range(EARLY, NT):
                 send_gu(w, kk, up=False)
 
-    for w in range(2):
-        for kk in range(1, NT):
-            send_gu(w, kk, down=False)
     pl.when(me < S - 1)(late_down)
 
     def pass_gu(kk, **sides):
         def one(j):
-            gz_copy(0, me, kk, j, j).wait_recv()
-            gz_copy(1, me, kk, j, j).wait_recv()
+            drain(gu.at[kk, pl.ds(0, half)], gzr.at[j, kk])
             gy_copy(j, kk, g).start()
 
         @pl.when(kk < n_me)
@@ -748,8 +751,7 @@
         af_copy(j, xpeer).start()
 
     def ready(j):
-        ac_copy(j, cpeer).wait_recv()
-        af_copy(j, far).wait_recv()
+        drain(xm.at[j, pl.ds(0, 2 * R)], acr.at[j])
         for r0 in range(0, T, R):
             rows_f = xm[j, pl.ds(r0, R)].astype(F32)
             at = pl.ds(pl.multiple_of(j * T + r0, R), R)
@@ -760,6 +762,9 @@
             pass_gu(kk, at=at)
 
     pass_gu(0)
+    for kk in range(1, NT):
+        send_gu(0, kk, down=False)
+        send_gu(1, kk, down=False)
     pass_gu(1, down=False)
     hand_on(me)
     planes(spread, at=(1,))
@@ -784,15 +789,15 @@
         return remote(hid_at(t, kk), hid_at(t, kk), hxs.at[kk], hxr.at[kk], "tp", xpeer)
 
     def hc_copy(t, kk):
-        return remote(hid_at(t, kk), hid_at(t, kk), hcs.at[kk], hcr.at[kk], "tp", cpeer)
+        return remote(hid_at(t, kk), hid_at(t, kk), hxs.at[kk], hcr.at[kk], "tp", cpeer)
 
     def hf_copy(t, kk):
-        return remote(hid_at(t, kk), hid_at(t, kk), hfs.at[kk], hfr.at[kk], "tp", cpeer)
+        return remote(hid_at(t, kk), hid_at(t, kk), hxs.at[kk], hcr.at[kk], "tp", cpeer)
 
     def tile(kk):
         own_gu(0, kk).wait()
         own_gu(1, kk).wait()
-        planes(lambda j: gy_copy(j, kk, 1 - g).wait_recv())
+        drain(gu.at[kk, pl.ds(0, (S - 1) * half)], gyr.at[kk])
         both = jnp.dot(xn[...], gu[kk], preferred_element_type=F32)
         gate, up = both[:, :128], both[:, 128:]
         hid[tp * NT + kk] = (gate / (1.0 + jnp.exp(-gate)) * up).astype(BF16)
@@ -806,7 +811,7 @@
     def pass_dn(j, at=range(TP)):
         def some(m):
             for f in at:
-                st = lax.rem(tp + TP - f, TP)
+                st = (tp, cpeer, xpeer, far)[f]
                 dz_copy(me, tp, j, st, m).wait_recv()
                 dy_copy(j, st, g, m).start()
 
@@ -817,26 +822,25 @@
     planes(pass_dn, at=(1,))
     with_tiles(pass_tile, at=(0,))
     with_tiles(tile, at=range(2, NT))
+    with_tiles(pass_tile, at=(1,))
     for f in range(TP):
-        if f == TP // 2:
-            with_tiles(pass_tile, at=range(1, NT))
+        if f == TP - 1:
+            with_tiles(pass_tile, at=range(2, NT))
         planes(lambda j: pass_dn(j, (f,)), at=range(2, S))
 
     def hid_ready(kk):
-        hc_copy(cpeer, kk).wait_recv()
-        hf_copy(far, kk).wait_recv()
+        drain(hid.at[pl.ds(0, 2)], hcr.at[kk])
 
     def rs_copy(j, dst, src):
-        return remote(us.at[j, dst], ur.at[j, src], rss.at[j, dst], rsr.at[j, src], "sp", dst)
+        return remote(us.at[j, dst], ur.at[j, src], rss.at[0], rsr.at[j], "sp", dst)
 
     def down(j, own=False):
         def some(m):
             if own:
                 own_dn(m).wait()
-                peers(lambda t: dp_copy(tp, t, m).wait_recv())
+                drain(dn.at[me, :, pl.ds(0, (TP - 1) * m * 128)], dzr.at[me, 0])
             else:
-                for t in range(TP):
-                    dy_copy(j, t, 1 - g, m).wait_recv()
+                drain(dn.at[j, pl.ds(0, Q // 2), pl.ds(0, TP * m * 128)], dyr.at[j])
             x = jnp.concatenate(
                 [hid[t * NT + kk] for t in range(TP) for kk in range(m)], axis=1
             )
@@ -851,16 +855,16 @@
         planes(down, at=(d,))
 
     def ox_copy(j, t):
-        return remote(zq.at[t, j], zq.at[t, j], oxs.at[j], oxr.at[j], "tp", xpeer)
+        return remote(zq.at[t, j], zq.at[t, j], oxs.at[0], oxr.at[j], "tp", xpeer)
 
     def oc_copy(j, t):
-        return remote(zq.at[t, j], zq.at[t, j], ocs.at[j], ocr.at[j], "tp", cpeer)
+        return remote(zq.at[t, j], zq.at[t, j], ocs.at[0], ocr.at[0], "tp", cpeer)
 
     def of_copy(j, t):
-        return remote(zq.at[t, j], zq.at[t, j], ofs.at[j], ofr.at[j], "tp", cpeer)
+        return remote(zq.at[t, j], zq.at[t, j], ocs.at[0], ocr.at[0], "tp", cpeer)
 
     def settle(j):
-        planes(lambda i: rs_copy(j, i, i).wait_recv())
+        drain(ur.at[j, pl.ds(0, S - 1)], rsr.at[j])
         total = us[j, me].astype(F32)
         for d in range(1, S):
             total += ur[j, lax.rem(me + d, S)].astype(F32)
@@ -868,18 +872,17 @@
         ox_copy(j, tp).start()
         oc_copy(j, tp).start()
 
-    for j in range(S):
+    order = sorted(range(S), key=lambda j: abs(2 * j + 1 - S))
+    for j in order:
         settle(j)
-    for j in range(S):
+    for j in order:
         ox_copy(j, xpeer).wait_recv()
         of_copy(j, xpeer).start()
-    for j in range(S):
-        oc_copy(j, cpeer).wait_recv()
-        of_copy(j, far).wait_recv()
+    drain(zq.at[pl.ds(0, 2)], ocr.at[0])
 
     def o_out(r):
         rows_r = pl.ds(r * R, R)
-        return pltpu.make_async_copy(ov.at[rows_r], out.at[rows_r], outs.at[r])
+        return pltpu.make_async_copy(ov.at[rows_r], out.at[rows_r], outs.at[0])
 
     for r in range(TP):
         rows_r = pl.ds(r * R, R)
@@ -889,46 +892,39 @@
         ov[rows_r] = (xm[me, rows_r].astype(F32) + og[...] * normalize(ffn)).astype(BF16)
         o_out(r).start()
 
-    peers(lambda t: hp_copy(t, tp).wait_send())
+    drain(hs.at[pl.ds(0, TP - 1)], hss.at[0])
     for j in range(S):
         pl.when(j <= me)(lambda: ends(j, lambda c: c.wait_send()))
-        ax_copy(j, tp).wait_send()
-        ac_copy(j, tp).wait_send()
-        af_copy(j, xpeer).wait_send()
-        ox_copy(j, tp).wait_send()
-        oc_copy(j, tp).wait_send()
-        of_copy(j, xpeer).wait_send()
-        planes(lambda i: rs_copy(j, i, me).wait_send())
-
+
+    drain(xm.at[:, pl.ds(0, R)], axs.at[0])
+    drain(xm.at[:, pl.ds(0, 2 * R)], acs.at[0])
+    drain(zq.at[0], oxs.at[0])
+    drain(zq.at[pl.ds(0, 2)], ocs.at[0])
+    drain(us.at[pl.ds(0, S - 1)], rss.at[0])
     planes(lambda i: az_copy(me, 0, i).wait_send(), up=False)
 
     def sent(i):
         for kk in range(NT):
-            for w in range(2):
-
-                @pl.when(kk < count(i))
-                def _(kk=kk, w=w):
-                    gz_copy(w, i, kk, me, i).wait_send()
+
+            @pl.when(kk < count(i))
+            def _(kk=kk):
+                drain(gu.at[kk, pl.ds(0, half)], gzs.at[i, kk])
 
         def some(m):
-            for t in range(TP):
-                dz_copy(i, t, me, tp, m).wait_send()
+            drain(dn.at[0, pl.ds(0, Q // 2), pl.ds(0, TP * m * 128)], dzs.at[i])
 
         tiles_of(i, some)
-        tiles_of(me, lambda m: [dy_copy(i, t, g, m).wait_send() for t in range(TP)])
+        tiles_of(me, lambda m: drain(dn.at[i, pl.ds(0, Q // 2), pl.ds(0, TP * m * 128)], dys.at[i]))
 
     planes(sent)
 
     def tile_sent(kk):
-        planes(lambda j: gy_copy(j, kk, g).wait_send())
-        hx_copy(tp, kk).wait_send()
-        hc_copy(tp, kk).wait_send()
-        hf_copy(xpeer, kk).wait_send()
+        drain(gu.at[kk, pl.ds(0, (S - 1) * half)], gys.at[kk])
+        drain(hid.at[pl.ds(0, 3)], hxs.at[kk])
 
     with_tiles(tile_sent)
-    tiles_of(me, lambda m: peers(lambda t: dp_copy(t, tp, m).wait_send()))
-    for r in range(TP):
-        o_out(r).wait()
+    tiles_of(me, lambda m: drain(dn.at[me, :, pl.ds(0, (TP - 1) * m * 128)], dzs.at[me]))
+    pltpu.make_async_copy(ov, out, outs.at[0]).wait()
 
 
 def gathered_call(S, TP, q, k, v, lgt, H, mg, fg, og, res, ow, gw, uw, dw):
@@ -969,25 +965,28 @@
             pltpu.VMEM((TP, S, T, Q), BF16),
             pltpu.VMEM((T, D), BF16),
             dma((3 + 2 * NT,)),
-            *pairs(S, 3),
-            *pairs(TP),
+            *pairs(S, 2),
+            *pairs(1),
             dma((2, S)),
             dma((S,)),
+            dma((1,)),
+            dma((S,)),
+            dma((1,)),
+            dma((S,)),
+            *pairs(S, NT),
+            *pairs(NT),
+            dma((S,)),
+            dma((S, TP)),
             *pairs(S),
-            *pairs(S),
-            *pairs(S),
-            *pairs(2, S, NT),
-            *pairs(S, NT),
-            *pairs(S, TP),
-            *pairs(S, TP),
-            *pairs(NT),
-            *pairs(NT),
-            *pairs(NT),
-            *pairs(S, S),
-            *pairs(S),
-            *pairs(S),
-            *pairs(S),
-            dma((TP,)),
+            dma((NT,)),
+            dma((NT,)),
+            dma((NT,)),
+            dma((1,)),
+            dma((S,)),
+            dma((1,)),
+            dma((S,)),
+            *pairs(1),
+            dma((1,)),
         ],
         compiler_params=pltpu.CompilerParams(
             collective_id=0, has_side_effects=True, vmem_limit_bytes=67043328 - 2**20

time: 94.1 us -> 92.8 us (0.986)
  the two profiles are of different devices: /device:TPU:1 before, /device:TPU:29 now
where the time goes in v4:
time: 92.8 us; the launch traced here: 92.6 us
  Pallas kernels  90.7 us (98%)
  local copies, waits for them, and re-layouts  1.88 us (2%)
    pallas_call x1, Pallas kernels, gathered_call(): pl.pallas_call(functools.partial(gathered, S, TP, H, base, extras), out_s...  90.7 us
    unnamed x1, local copies, waits for them, and re-layouts  1.88 us

profile of v4, /device:TPU:29, one launch (start us, length us, event | category | flops | bytes accessed | tf_op | source)
XLA Modules:
  0.0 92.6 jit_solution(18307276796419182759)
XLA Ops:
  0.0 90.7 %shard_map.118 = bf16[128,2048]{1,0:T(8,128)(2,1)} custom-call(bf16[128,256]{1,0:T(8,128)(2,1)} %q.1, bf16[128,256]{1,0:T(8,128)(2,1)} %k.1, bf16[128,256]{1,0:T(8,128)(2,1)} %v.1, bf16[2,128]{1,0:T(2,128)(2,1)} %bitcast.7, f32[1,2048]{1,0:T(1,128)} %bitcast.4, f32[1,2048]{1,0:T(1,128)} %bitcast.5, f32[1,2048]{1,0:T(1,128)} %bitcast.6, ...), custom_call_target="tpu_custom_call" | custom-call | tf_op jit(solution)/shard_map/pallas_call | solution.py:942
  90.7 1.9 %copy.14 = bf16[128,2048]{1,0:T(8,128)(2,1)} copy(bf16[128,2048]{1,0:T(8,128)(2,1)} %shard_map.118) | data formatting | bytes 1048576

commit v5 on v4

--- a/solution.py
+++ b/solution.py
@@ -615,9 +615,9 @@
         for f in range(1, TP):
             body(lax.rem(tp + f, TP))
 
-    def send_dn(i):
+    def send_dn(i, to=(tp, cpeer, xpeer, far)):
         def some(m):
-            for t in (tp, cpeer, xpeer, far):
+            for t in to:
                 dz_copy(i, t, me, tp, m).start()
 
         tiles_of(i, some)
@@ -720,7 +720,22 @@
         return remote(piece_of(j, t), piece_of(j, t), acs.at[0], acr.at[j], "tp", cpeer)
 
     ends(me, lambda c: c.start())
-    planes(lambda i: az_copy(me, 0, i).start(), up=False, at=range(S - 1, 0, -1))
+    def own_left(body):
+        @pl.when(me == S - 1)
+        def _():
+            for i in range(S - 1):
+                body(az_copy(me, 0, i))
+
+        @pl.when((me < S - 1) & (me > 0))
+        def _():
+            body(az_copy(me, 0, me - 1))
+
+    def pass_left(j, body):
+        @pl.when((j > me) & (j < S - 1) & (me > 0))
+        def _():
+            body(az_copy(j, 2, me - 1))
+
+    own_left(lambda c: c.start())
     ax_copy(me, tp).start()
     ac_copy(me, tp).start()
 
@@ -743,6 +758,7 @@
     def spread(j):
         az_copy(j, 1, me).wait_recv()
         ends(j, lambda c: c.start())
+        pass_left(j, lambda c: c.start())
         ax_copy(j, tp).start()
         ac_copy(j, tp).start()
 
@@ -772,11 +788,13 @@
     pl.when(me == S - 1)(late_down)
     ready(me)
     planes(spread, at=(2,))
+    pl.when(2 * me >= S)(lambda: planes(lambda i: send_dn(i, (tp, cpeer))))
     pass_late((1,))
     planes(hand_on, at=(2,))
     planes(spread, at=range(3, S))
     pass_late((2,))
-    planes(send_dn)
+    pl.when(2 * me < S)(lambda: planes(send_dn))
+    pl.when(2 * me >= S)(lambda: planes(lambda i: send_dn(i, (xpeer, far))))
     planes(hand_on, at=range(3, S))
     pass_gu(1, up=False)
     pass_late(range(3, S))
@@ -901,7 +919,8 @@
     drain(zq.at[0], oxs.at[0])
     drain(zq.at[pl.ds(0, 2)], ocs.at[0])
     drain(us.at[pl.ds(0, S - 1)], rss.at[0])
-    planes(lambda i: az_copy(me, 0, i).wait_send(), up=False)
+    own_left(lambda c: c.wait_send())
+    planes(lambda j: pass_left(j, lambda c: c.wait_send()), down=False)
 
     def sent(i):
         for kk in range(NT):
@@ -967,7 +986,7 @@
             dma((3 + 2 * NT,)),
             *pairs(S, 2),
             *pairs(1),
-            dma((2, S)),
+            dma((3, S)),
             dma((S,)),
             dma((1,)),
             dma((S,)),

time: 92.8 us -> 92.2 us (level)
  the two profiles are of different devices: /device:TPU:29 before, /device:TPU:1 now
where the time goes in v5:
time: 92.2 us; the launch traced here: 91.9 us
  Pallas kernels  90 us (98%)
  local copies, waits for them, and re-layouts  1.88 us (2%)
    pallas_call x1, Pallas kernels, gathered_call(): pl.pallas_call(functools.partial(gathered, S, TP, H, base, extras), out_s...  90 us
    unnamed x1, local copies, waits for them, and re-layouts  1.88 us

profile of v5, /device:TPU:1, one launch (start us, length us, event | category | flops | bytes accessed | tf_op | source)
XLA Modules:
  0.0 91.9 jit_solution(4614633508597834095)
XLA Ops:
  0.0 90.0 %shard_map.118 = bf16[128,2048]{1,0:T(8,128)(2,1)} custom-call(bf16[128,256]{1,0:T(8,128)(2,1)} %q.1, bf16[128,256]{1,0:T(8,128)(2,1)} %k.1, bf16[128,256]{1,0:T(8,128)(2,1)} %v.1, bf16[2,128]{1,0:T(2,128)(2,1)} %bitcast.7, f32[1,2048]{1,0:T(1,128)} %bitcast.4, f32[1,2048]{1,0:T(1,128)} %bitcast.5, f32[1,2048]{1,0:T(1,128)} %bitcast.6, ...), custom_call_target="tpu_custom_call" | custom-call | tf_op jit(solution)/shard_map/pallas_call | solution.py:961
  90.0 1.9 %copy.14 = bf16[128,2048]{1,0:T(8,128)(2,1)} copy(bf16[128,2048]{1,0:T(8,128)(2,1)} %shard_map.118) | data formatting | bytes 1048576

commit v6 on v5

--- a/solution.py
+++ b/solution.py
@@ -781,9 +781,10 @@
     for kk in range(1, NT):
         send_gu(0, kk, down=False)
         send_gu(1, kk, down=False)
+    planes(spread, up=False, at=(1,))
     pass_gu(1, down=False)
     hand_on(me)
-    planes(spread, at=(1,))
+    planes(spread, down=False, at=(1,))
     planes(hand_on, at=(1,))
     pl.when(me == S - 1)(late_down)
     ready(me)

time: 92.2 us -> 92.2 us (level)
  no operation moved by 1% of the time
where the time goes in v6:
time: 92.2 us; the launch traced here: 91.9 us
  Pallas kernels  90 us (98%)
  local copies, waits for them, and re-layouts  1.88 us (2%)
    pallas_call x1, Pallas kernels, gathered_call(): pl.pallas_call(functools.partial(gathered, S, TP, H, base, extras), out_s...  90 us
    unnamed x1, local copies, waits for them, and re-layouts  1.88 us

profile of v6, /device:TPU:1, one launch (start us, length us, event | category | flops | bytes accessed | tf_op | source)
XLA Modules:
  0.0 91.9 jit_solution(7973658207869624939)
XLA Ops:
  0.0 90.0 %shard_map.118 = bf16[128,2048]{1,0:T(8,128)(2,1)} custom-call(bf16[128,256]{1,0:T(8,128)(2,1)} %q.1, bf16[128,256]{1,0:T(8,128)(2,1)} %k.1, bf16[128,256]{1,0:T(8,128)(2,1)} %v.1, bf16[2,128]{1,0:T(2,128)(2,1)} %bitcast.7, f32[1,2048]{1,0:T(1,128)} %bitcast.4, f32[1,2048]{1,0:T(1,128)} %bitcast.5, f32[1,2048]{1,0:T(1,128)} %bitcast.6, ...), custom_call_target="tpu_custom_call" | custom-call | tf_op jit(solution)/shard_map/pallas_call | solution.py:962
  90.0 1.9 %copy.14 = bf16[128,2048]{1,0:T(8,128)(2,1)} copy(bf16[128,2048]{1,0:T(8,128)(2,1)} %shard_map.118) | data formatting | bytes 1048576
